TPU v7x, 256 devices: a whole 4x4x8 slice. The times are simulated.
256 devices in a mesh: sp: 16 (over y, x), dp: 16 (over z, core).
Axes of the slice: x: 4, y: 4, z: 8, core: 2. Of those that a mesh axis runs over, the one named last changes fastest.
Arguments:
- tokens: bfloat16 [16, 4096, 2048], P('dp', 'sp'), may hold values from -200 to 200
- w_qdown: bfloat16 [2048, 512], P('dp'), may hold values from -0.125 to 0.125
- w_kvdown: bfloat16 [2048, 512], P('dp'), may hold values from -0.125 to 0.125
- w_rotary: bfloat16 [2048, 64], replicated, may hold values from -0.125 to 0.125
- q_gain: float32 [512], replicated, may hold values from 0.1 to 1.9
- kv_gain: float32 [512], replicated, may hold values from 0.1 to 1.9
- w_qup: bfloat16 [512, 3072], P('dp'), may hold values from -1 to 1
- w_kvup: bfloat16 [512, 4096], P('dp'), may hold values from -1 to 1
- w_out: bfloat16 [2048, 2048], P(None, 'dp'), may hold values from -0.125 to 0.125
- out_gain: float32 [2048], replicated, may hold values from 0.1 to 1.9
Outputs:
- mixed: bfloat16 [16, 4096, 2048], P('dp', 'sp')
All inputs are finite; a program needn't handle non-finite values.
Results may differ from a plain program's by a relative error of at most 0.01.
The roundings to bfloat16 on the way count: a program that leaves them out, or rounds other values in their place, can miss the bound.
Values may be sent and summed in bfloat16 or wider, within the bound.
A program may use at most 128 MiB of HBM per device.

v0:
```python
import math

import jax
import jax.numpy as jnp
from jax import lax
from jax.sharding import PartitionSpec as P

HEADS = 16
NOPE = 128
ROPE = 64
VDIM = 128


EPSILON = 1e-06
THETA = 10000.0


def in_one_piece(arrays, axis, dim, along):
    both = jnp.concatenate(arrays, axis=along)
    filled, at, gathered = (lax.all_gather(both, axis, axis=dim, tiled=True), 0, [])
    for a in arrays:
        gathered.append(lax.slice_in_dim(filled, at, at + a.shape[along], axis=along))
        at += a.shape[along]
    return tuple(gathered)


def norm_rows(values, gain):
    scale = lax.rsqrt(jnp.mean(values * values, axis=-1, keepdims=True) + EPSILON)
    return values * scale * gain


def rotate(values, cosine, sine):
    half = values.shape[-1] // 2
    first = values[..., :half]
    second = values[..., half:]
    return jnp.concatenate(
        [first * cosine - second * sine, second * cosine + first * sine], axis=-1
    )


def turn_tables(offset, count):
    positions = (offset + jnp.arange(count)).astype(jnp.float32)
    freqs = THETA ** (-jnp.arange(0, ROPE, 2).astype(jnp.float32) / ROPE)
    angles = positions[:, None] * freqs[None, :]
    return (jnp.cos(angles), jnp.sin(angles))


def make_queries(q_full, cosine, sine, heads_here):
    rows = q_full.shape[0]
    shaped = q_full.reshape(rows, heads_here, NOPE + ROPE)
    turned = rotate(shaped[..., NOPE:], cosine[:, None, :], sine[:, None, :])
    joined = jnp.concatenate([shaped[..., :NOPE], turned], axis=-1)
    return joined.reshape(rows, heads_here * (NOPE + ROPE)).astype(jnp.bfloat16)


def attend(query_heads, keyval_heads, key_rot, heads_here):
    length = query_heads.shape[0]
    block = math.gcd(length, 512)
    scaling = (NOPE + ROPE) ** (-0.5)
    queries = query_heads.reshape(length, heads_here, NOPE + ROPE)
    keyval = keyval_heads.reshape(length, heads_here, NOPE + VDIM)
    keys_all = keyval[..., :NOPE]
    values_all = keyval[..., NOPE:]
    outputs = []
    for begin in range(0, length, block):
        finish = begin + block
        query_block = queries[begin:finish]
        scores = jnp.einsum(
            "qhd,khd->hqk",
            query_block[..., :NOPE],
            keys_all[:finish],
            preferred_element_type=jnp.float32,
        )
        scores = scores + jnp.einsum(
            "qhd,kd->hqk",
            query_block[..., NOPE:],
            key_rot[:finish],
            preferred_element_type=jnp.float32,
        )
        scores = scores * scaling
        query_pos = begin + jnp.arange(block)
        key_pos = jnp.arange(finish)
        allowed = key_pos[None, :] <= query_pos[:, None]
        scores = jnp.where(allowed[None], scores, -jnp.inf)
        top = jnp.max(scores, axis=-1, keepdims=True)
        expo = jnp.exp(scores - top)
        weights = (expo / jnp.sum(expo, axis=-1, keepdims=True)).astype(jnp.bfloat16)
        attended = jnp.einsum(
            "hqk,khd->qhd", weights, values_all[:finish], preferred_element_type=jnp.float32
        )
        outputs.append(attended.astype(jnp.bfloat16))
    return jnp.concatenate(outputs, axis=0).reshape(length, heads_here * VDIM)


def body(tokens, w_qdown, w_kvdown, w_rotary, q_gain, kv_gain, w_qup, w_kvup, w_out, out_gain):
    own_rows = tokens[0]
    tok_count = own_rows.shape[0]
    sp_count = lax.axis_size("sp")
    sp_place = lax.axis_index("sp")
    length = tok_count * sp_count
    heads_here = HEADS // sp_count
    pieces = in_one_piece((w_qdown, w_kvdown), "dp", 0, 1)
    q_lat = jnp.dot(own_rows, pieces[0], preferred_element_type=jnp.float32)
    kv_lat = jnp.dot(own_rows, pieces[1], preferred_element_type=jnp.float32)
    q_norm = norm_rows(q_lat, q_gain).astype(jnp.bfloat16)
    kv_norm = norm_rows(kv_lat, kv_gain).astype(jnp.bfloat16)
    own_cos, own_sin = turn_tables(sp_place * tok_count, tok_count)
    key_rot = rotate(
        jnp.dot(own_rows, w_rotary, preferred_element_type=jnp.float32), own_cos, own_sin
    ).astype(jnp.bfloat16)
    q_all, kv_all, rot_all = in_one_piece((q_norm, kv_norm, key_rot), "sp", 0, 1)
    q_width = heads_here * (NOPE + ROPE)
    kv_width = heads_here * (NOPE + VDIM)
    q_columns = lax.dynamic_slice_in_dim(w_qup, sp_place * q_width, q_width, 1)
    kv_columns = lax.dynamic_slice_in_dim(w_kvup, sp_place * kv_width, kv_width, 1)
    pieces = in_one_piece((q_columns, kv_columns), "dp", 0, 1)
    q_full = jnp.dot(q_all, pieces[0], preferred_element_type=jnp.float32)
    kv_full = jnp.dot(kv_all, pieces[1], preferred_element_type=jnp.float32)
    all_cos, all_sin = turn_tables(0, length)
    query_heads = make_queries(q_full, all_cos, all_sin, heads_here)
    keyval_heads = kv_full.astype(jnp.bfloat16)
    attended = attend(query_heads, keyval_heads, rot_all, heads_here)
    merged = lax.all_to_all(attended, "sp", split_axis=0, concat_axis=1, tiled=True)
    proj = jnp.dot(
        merged, lax.all_gather(w_out, "dp", axis=1, tiled=True), preferred_element_type=jnp.float32
    )
    mixed = norm_rows(proj, out_gain).astype(jnp.bfloat16)
    return mixed[None]


def solution(mesh):
    in_specs = (
        P("dp", "sp", None),
        P("dp", None),
        P("dp", None),
        P(),
        P(),
        P(),
        P("dp", None),
        P("dp", None),
        P(None, "dp"),
        P(),
    )
    out_specs = P("dp", "sp", None)
    return jax.shard_map(body, mesh=mesh, in_specs=in_specs, out_specs=out_specs, check_vma=False)
```

profile of v0, /device:TPU:32, one launch (start us, length us, event | category | flops | bytes accessed | tf_op | source)
XLA Modules:
  0.0 231.6 jit_solution(769725246544850834)
XLA Ops:
  6.5 1.8 pad_maximum_fusion.1
  8.3 0.0 all-gather.4.cloned.1.call-update
  8.3 0.0 all-gather.6.cloned.1.call-start
  8.4 1.4 fusion.105
  9.8 0.2 fusion.166
  10.0 0.0 copy-start.7
  10.1 0.0 copy-start.8
  10.1 43.4 %all-gather.4.cloned.1.call-done = bf16[2048,1024]{1,0:T(8,128)(2,1)} async-done(((bf16[128,1024]{1,0:T(8,128)(2,1)}), bf16[2048,1024]{1,0:T(8,128)(2,1)}) %all-gather.4.cloned.1.call-update) | async-done | bytes 4194320 | tf_op jit(solution)/shard_map/all_gather | solution.py:20
  53.5 2.5 %multiply_reduce_fusion.2 = (f32[256]{0:T(256)S(1)}, f32[512,256]{1,0:T(8,128)S(1)}) fusion(bf16[1,256,2048]{2,1,0:T(8,128)(2,1)S(1)} %copy-done, bf16[2048,1024]{1,0:T(8,128)(2,1)} %all-gather.4.cloned.1.call-done), kind=kOutput, calls=%fused_computation.159 | convolution fusion | flops 537132800 | bytes 3671040 | tf_op jit(solution)/shard_map/dot_general | solution.py:103
  56.0 0.3 copy-done.9
  56.3 0.8 multiply_reduce_fusion.1
  57.1 0.2 fusion.128
  57.3 0.8 pad_maximum_fusion
  58.1 0.0 all-gather.6.cloned.1.call-update
  58.2 0.0 all-gather.8.cloned.1.call-start
  58.2 0.7 all-gather.8.cloned.1.call-update
  59.0 0.7 constant_dynamic-slice_fusion
  59.7 0.8 constant_dynamic-slice_fusion.1
  60.5 0.1 pad_maximum_fusion.3
  60.6 16.3 %all_gather.14 = bf16[512,448]{1,0:T(8,128)(2,1)S(1)} all-gather(bf16[32,448]{1,0:T(8,128)(2,1)S(1)} %pad_maximum_fusion.3), channel_id=1, replica_groups=mesh['sp'=16,'dp'=16] {'dp'}, dimensions={0}, use_global_device_ids=true | all-gather | bytes 487424 | tf_op jit(solution)/shard_map/all_gather | solution.py:20
  76.9 65.1 %all-gather.6.cloned.1.call-done = bf16[4096,1088]{0,1:T(8,128)(2,1)} async-done(((bf16[256,1088]{0,1:T(8,128)(2,1)}), bf16[4096,1088]{0,1:T(8,128)(2,1)}) %all-gather.6.cloned.1.call-update) | async-done | bytes 8912912 | tf_op jit(solution)/shard_map/all_gather | solution.py:20
  141.9 3.4 %fusion.177 = (bf16[4096,1,192]{0,2,1:T(8,128)(2,1)S(1)}, f32[4096,1,192]{0,2,1:T(8,128)S(1)}) fusion(bf16[512,448]{1,0:T(8,128)(2,1)S(1)} %all_gather.14, bf16[4096,1088]{0,1:T(8,128)(2,1)} %all-gather.6.cloned.1.call-done), kind=kOutput, calls=%fused_computation.238 | convolution fusion | flops 806092800 | bytes 9175040 | tf_op jit(solution)/shard_map/dot_general | solution.py:117
  145.3 2.5 %fusion.120 = (bf16[4096,1,32]{0,2,1:T(8,128)(2,1)S(1)}, bf16[4096,1,32]{0,2,1:T(8,128)(2,1)S(1)}) fusion(f32[4096,1,192]{0,2,1:T(8,128)S(1)} %get-tuple-element.14, f32[32]{0:T(128)S(1)} %multiply_power_fusion, f32[4096]{0:T(1024)S(1)} %iota_convert_fusion), kind=kLoop, calls=%fused_computation.149 | loop fusion | flops 1179648 | bytes 1589376 | tf_op jit(solution)/shard_map/convert.2
  147.8 1.4 fusion.11
  149.2 0.3 convolution_bitcast_fusion.3
  149.5 0.6 convolution_bitcast_fusion.2
  150.1 0.3 fusion.178
  150.4 0.2 fusion.109
  150.6 0.5 fusion.131
  151.1 0.7 fusion.179
  151.8 0.5 fusion.38
  152.3 1.0 fusion.180
  153.3 0.6 fusion.27
  153.9 1.1 fusion.63
  155.0 0.7 fusion.122
  155.8 1.2 fusion.181
  157.0 2.0 copy-done.2
  159.0 0.7 fusion.19
  159.7 0.9 fusion.116
  160.6 1.5 fusion.182
  162.1 0.8 fusion.12
  162.9 1.0 fusion.111
  164.0 2.0 fusion.183
  166.0 1.0 fusion.8
  167.0 1.3 fusion.71
  168.3 1.1 fusion.110
  169.5 2.9 %fusion.184 = (f32[512]{0:T(512)S(1)}, f32[1,512,3584]{2,1,0:T(8,128)S(1)}) fusion(bf16[4096,1,32]{0,2,1:T(8,128)(2,1)S(1)} %get-tuple-element.5, bf16[4096,1,32]{0,2,1:T(8,128)(2,1)S(1)} %get-tuple-element.6, bf16[4096,1088]{0,1:T(8,128)(2,1)} %all-gather.6.cloned.1.call-done, f32[512,3584]{1,0:T(8,128)S(1)} %fusion.110, s32[512]{0:T(512)S(1)} %iota_add_fusion.1), kind=kOutput, calls=%fused_computation.245 | convolution fusion | flops 244186624 | bytes 15667200 | tf_op jit(solution)/shard_map/qhd,kd->hqk/dot_general | solution.py:74
  172.4 1.1 fusion.5
  173.5 1.3 fusion.103
  174.8 3.2 %fusion.185 = (f32[512]{0:T(512)S(1)}, f32[1,512,4096]{2,1,0:T(8,128)S(1)}) fusion(bf16[4096,1,32]{0,2,1:T(8,128)(2,1)S(1)} %get-tuple-element.5, bf16[4096,1,32]{0,2,1:T(8,128)(2,1)S(1)} %get-tuple-element.6, bf16[4096,1088]{0,1:T(8,128)(2,1)} %all-gather.6.cloned.1.call-done, f32[512,4096]{1,0:T(8,128)S(1)} %fusion.103, s32[512]{0:T(512)S(1)} %iota_add_fusion), kind=kOutput, calls=%fused_computation.246 | convolution fusion | flops 279051776 | bytes 17829888 | tf_op jit(solution)/shard_map/qhd,kd->hqk/dot_general | solution.py:74
  178.0 1.3 fusion.2
  179.3 3.6 %fusion.99 = bf16[4096,1,128]{0,2,1:T(8,128)(2,1)} fusion(bf16[4096,1,128]{0,2,1:T(8,128)(2,1)} %fusion.71, f32[512]{0:T(512)S(1)} %fusion.27, f32[1,512,1536]{2,1,0:T(8,128)} %copy-done.4, f32[512]{0:T(512)S(1)} %get-tuple-element.19, bf16[4096,1,256]{2,0,1:T(8,128)(2,1)S(1)} %fusion.11), kind=kOutput, calls=%fused_computation.102 | convolution fusion | flops 203751424 | bytes 3674112 | tf_op jit(solution)/shard_map/hqk,khd->qhd/dot_general | solution.py:88
  182.9 2.0 fusion.67
  184.9 1.9 fusion.93
  186.8 2.1 fusion.87
  188.8 2.2 fusion.81
  191.1 2.4 %fusion.75 = bf16[4096,1,128]{0,2,1:T(8,128)(2,1)} fusion(bf16[4096,1,128]{0,2,1:T(8,128)(2,1)} %fusion.81, f32[512]{0:T(512)S(1)} %fusion.2, f32[1,512,4096]{2,1,0:T(8,128)S(1)} %get-tuple-element.30, f32[512]{0:T(512)S(1)} %get-tuple-element.29, bf16[4096,1,256]{2,0,1:T(8,128)(2,1)S(1)} %fusion.11), kind=kOutput, calls=%fused_computation.94 | convolution fusion | flops 543227904 | bytes 9572352 | tf_op jit(solution)/shard_map/hqk,khd->qhd/dot_general | solution.py:88
  193.5 1.5 copy.33
  195.0 1.3 copy.25
  196.3 4.9 %all-to-all-start = ((bf16[16,256,128]{1,2,0:T(8,128)(2,1)}), bf16[16,256,128]{1,2,0:T(8,128)(2,1)S(1)}, u32[]{:S(2)}, u32[]{:S(2)}) async-start(bf16[16,256,128]{1,2,0:T(8,128)(2,1)} %copy.25), calls=%async_computation | async-start | bytes 2097152 | tf_op jit(solution)/shard_map/all_to_all | solution.py:123
  201.3 6.6 %all-gather.8.cloned.1.call-done = bf16[2048,2048]{1,0:T(8,128)(2,1)} async-done(((bf16[2048,128]{1,0:T(8,128)(2,1)}), bf16[2048,2048]{1,0:T(8,128)(2,1)}) %all-gather.8.cloned.1.call-update) | async-done | bytes 8388624 | tf_op jit(solution)/shard_map/all_gather | solution.py:125
  207.9 9.6 %all-to-all-done = bf16[16,256,128]{1,2,0:T(8,128)(2,1)S(1)} async-done(((bf16[16,256,128]{1,2,0:T(8,128)(2,1)}), bf16[16,256,128]{1,2,0:T(8,128)(2,1)S(1)}, u32[]{:S(2)}, u32[]{:S(2)}) %all-to-all-start) | async-done | bytes 1048608 | tf_op jit(solution)/shard_map/all_to_all | solution.py:123
  217.5 5.9 %multiply_reduce_fusion = (f32[256]{0:T(256)S(1)}, f32[256,2048]{1,0:T(8,128)S(1)}) fusion(bf16[256,2048]{0,1:T(8,128)(2,1)S(1)} %bitcast.336, bf16[2048,2048]{1,0:T(8,128)(2,1)} %all-gather.8.cloned.1.call-done), kind=kOutput, calls=%fused_computation.67 | convolution fusion | flops 2148531968 | bytes 11535360 | tf_op jit(solution)/shard_map/dot_general | solution.py:124
  223.4 1.2 fusion.102
  (30 shorter events, 0.1 us)
Async XLA Ops:
  6.5 1.9 copy-start
  6.5 46.9 %all-gather.4.cloned.1.call-start = ((), (), s32[]{:S(2)}) async-start(), calls=%async_computation.1 | async-start | bytes 4456448 | tf_op jit(solution)/shard_map/all_gather | solution.py:20
  8.3 133.6 %all-gather.6.cloned.1.call-start = ((), (), s32[]{:S(2)}) async-start(), calls=%async_computation.2 | async-start | bytes 9469952 | tf_op jit(solution)/shard_map/all_gather | solution.py:20
  10.0 47.0 %copy-start.7 = (f32[512]{0:T(512)S(1)}, f32[512]{0:T(512)}, u32[]{:S(2)}) copy-start(f32[512]{0:T(512)} %param.14) | copy-start | bytes 6148
  10.1 47.0 %copy-start.8 = (f32[512]{0:T(512)S(1)}, f32[512]{0:T(512)}, u32[]{:S(2)}) copy-start(f32[512]{0:T(512)} %param.15) | copy-start | bytes 6148
  53.5 2.8 %copy-start.9 = (bf16[2048,1024]{1,0:T(8,128)(2,1)S(1)}, bf16[2048,1024]{1,0:T(8,128)(2,1)}, u32[]{:S(2)}) copy-start(bf16[2048,1024]{1,0:T(8,128)(2,1)} %all-gather.4.cloned.1.call-done) | copy-start | bytes 12582916
  58.2 149.7 %all-gather.8.cloned.1.call-start = ((), (), s32[]{:S(2)}) async-start(), calls=%async_computation.3 | async-start | bytes 8912896 | tf_op jit(solution)/shard_map/all_gather | solution.py:125
  141.9 5.9 %copy-start.5 = (bf16[4096,1088]{0,1:T(8,128)(2,1)S(1)}, bf16[4096,1088]{0,1:T(8,128)(2,1)}, u32[]{:S(2)}) copy-start(bf16[4096,1088]{0,1:T(8,128)(2,1)} %all-gather.6.cloned.1.call-done) | copy-start | bytes 26738692
  153.3 3.7 %copy-start.4 = (f32[1,512,1536]{2,1,0:T(8,128)}, f32[1,512,1536]{2,1,0:T(8,128)S(1)}, u32[]{:S(2)}) copy-start(f32[1,512,1536]{2,1,0:T(8,128)S(1)} %get-tuple-element.20) | copy-start | bytes 9437188
  157.0 2.0 copy-start.2
  179.3 3.6 %copy-start.3 = (f32[1,512,2048]{2,1,0:T(8,128)S(1)}, f32[1,512,2048]{2,1,0:T(8,128)}, u32[]{:S(2)}) copy-start(f32[1,512,2048]{2,1,0:T(8,128)} %copy-done.2) | copy-start | bytes 12582916
  196.3 21.1 %all-to-all-start = ((bf16[16,256,128]{1,2,0:T(8,128)(2,1)}), bf16[16,256,128]{1,2,0:T(8,128)(2,1)S(1)}, u32[]{:S(2)}, u32[]{:S(2)}) async-start(bf16[16,256,128]{1,2,0:T(8,128)(2,1)} %copy.25), calls=%async_computation | async-start | bytes 2097152 | tf_op jit(solution)/shard_map/all_to_all | solution.py:123
  217.5 5.9 %copy-start.6 = (f32[2048]{0:T(1024)S(1)}, f32[2048]{0:T(1024)}, u32[]{:S(2)}) copy-start(f32[2048]{0:T(1024)} %param.19) | copy-start | bytes 24580
  217.5 7.1 %copy-start.1 = (bf16[1,256,2048]{2,1,0:T(8,128)(2,1)S(1)}, bf16[1,256,2048]{2,1,0:T(8,128)(2,1)}, u32[]{:S(2)}) copy-start(bf16[1,256,2048]{2,1,0:T(8,128)(2,1)} %param.10) | copy-start | bytes 3145732
Sparse Core Ops, SparseCore 0:
  9.2 44.2 all-gather.3
  58.3 83.6 all-gather.5
  143.7 64.1 all-gather.7
where the time goes:
time: 236 us; the launch traced here: 232 us
  waiting for transfers between devices  125 us (53%)
  matrix products  51.4 us (22%)
  blocking collectives  16.3 us (7%)
  between operations  13.8 us (6%)
  other arithmetic  13.1 us (6%)
  local copies, waits for them, and re-layouts  6.63 us (3%)
  starting transfers between devices  5 us (2%)
    all_gather x2, waiting for transfers between devices, in_one_piece(): lax.all_gather(both, axis, axis=dim, tiled=True)  108 us
    dot_general x8, matrix products, attend(): jnp.einsum('hqk,khd->qhd', weights, values_all[:finish], preferred_elemen...  16.7 us
    all_gather x1, blocking collectives, in_one_piece(): lax.all_gather(both, axis, axis=dim, tiled=True)  16.3 us
    dot_general x8, matrix products, attend(): jnp.einsum('qhd,kd->hqk', query_block[..., NOPE:], key_rot[:finish], pref...  13 us
    all_to_all x1, waiting for transfers between devices, body(): lax.all_to_all(attended, 'sp', split_axis=0, concat_axis=1, tiled=True)  9.58 us
    all_gather x1, waiting for transfers between devices, body(): lax.all_gather(w_out, 'dp', axis=1, tiled=True)  6.62 us
    dot_general x8, matrix products, attend(): jnp.einsum('qhd,khd->hqk', query_block[..., :NOPE], keys_all[:finish], pr...  6.39 us
    reduce_sum x8, other arithmetic, attend(): jnp.sum(expo, axis=-1, keepdims=True)  6.23 us
  transfers between devices with their start and end apart: 4, of which 4 were waited for; matrix products, arithmetic and copies ran while one was open for 24% of the time, Pallas kernels for 0%

commit v1 on v0

v1 whole, which is shorter than its diff:
```python
import functools

import jax
import jax.numpy as jnp
import numpy as np
from jax import lax
from jax.experimental import pallas as pl
from jax.experimental.pallas import tpu as pltpu
from jax.sharding import PartitionSpec as P

HEADS = 16
NOPE = 128
ROPE = 64
VDIM = 128
D = 2048
RANK = 512
LENGTH = 4096
BLOCK = 256
EPSILON = 1e-06
THETA = 10000.0
LOG2E = 1.4426950408889634
SCALE = (NOPE + ROPE) ** (-0.5) * LOG2E
MESH = pl.DeviceIdType.MESH
BF16 = jnp.bfloat16
F32 = jnp.float32
Q_WIDTH = 4 * NOPE
R_WIDTH = 4 * ROPE
UP_WIDTH = Q_WIDTH + R_WIDTH + 4 * (NOPE + VDIM)
A_ROWS = 96
KV_ROWS = BLOCK + 32


def turn_table():
    positions = np.arange(LENGTH).astype(np.float32)
    freqs = np.float32(THETA) ** (-np.arange(0, ROPE, 2).astype(np.float32) / np.float32(ROPE))
    angles = positions[:, None] * freqs[None, :].astype(np.float32)
    cosine, sine = np.cos(angles), np.sin(angles)
    return np.concatenate([cosine, cosine, -sine, sine], axis=1).astype(np.float32)


def dot(a, b):
    return jnp.dot(a, b, preferred_element_type=F32)


def kernel(
    tok_hbm, wq_hbm, wkv_hbm, wrot, q_gain, kv_gain, wqup_hbm, wkvup_hbm, wout_hbm, out_gain, tab_hbm,
    out_ref,
    tk, pt, lhs, wd, part_send, part_recv, kvb, qb, wqs, wup, wo, tab, kcat, vbuf, qcat, acc, mbuf, lbuf,
    osend, orecv, send_sems, recv_sems, local_sems,
):
    sp, dp = lax.axis_index("sp"), lax.axis_index("dp")
    y, x = lax.div(sp, 4), lax.rem(sp, 4)
    z, c = lax.div(dp, 2), lax.rem(dp, 2)

    def m4(v):
        return lax.rem(v + 8, 4)

    def m8(v):
        return lax.rem(v + 16, 8)

    def plane(yy, xx):
        return (m4(yy) * 4 + m4(xx), dp)

    def along(zz):
        return (sp, m8(zz) * 2 + c)

    partner = (sp, z * 2 + (1 - c))
    xp, xm, yp, ym = plane(y, x + 1), plane(y, x - 1), plane(y + 1, x), plane(y - 1, x)
    zp, zm = along(z + 1), along(z - 1)

    local = [
        pltpu.make_async_copy(wq_hbm, wd.at[z, :, pl.ds(0, RANK)], local_sems.at[0]),
        pltpu.make_async_copy(wkv_hbm, wd.at[z, :, pl.ds(RANK, RANK)], local_sems.at[1]),
        pltpu.make_async_copy(tok_hbm, tk, local_sems.at[2]),
        pltpu.make_async_copy(
            wqup_hbm.at[:, pl.ds(pl.multiple_of(y * 768, 128), 768)], wqs, local_sems.at[3]
        ),
        pltpu.make_async_copy(
            wkvup_hbm.at[:, pl.ds(pl.multiple_of(y * 1024, 128), 1024)],
            wup.at[dp, :, pl.ds(Q_WIDTH + R_WIDTH, 1024)],
            local_sems.at[4],
        ),
        pltpu.make_async_copy(
            wout_hbm, wo.at[:, pl.ds(pl.multiple_of(dp * 128, 128), 128)], local_sems.at[5]
        ),
    ]
    for i in range(4):
        local.append(
            pltpu.make_async_copy(
                tab_hbm.at[pl.ds(pl.multiple_of(i * 1024 + x * 256, 256), 256)], tab.at[i], local_sems.at[6 + i]
            )
        )
    for copy in local:
        copy.start()

    barrier = pltpu.get_barrier_semaphore()
    for peer in (xp, xm, yp, ym, plane(y + 2, x), zp, zm, partner):
        pl.semaphore_signal(barrier, inc=1, device_id=peer, device_id_type=MESH)
    pl.semaphore_wait(barrier, 8)

    count = [0]
    started = []

    def remote(src, dst, peer, incoming):
        k = count[0]
        count[0] += 1
        out = pltpu.make_async_remote_copy(
            src_ref=src, dst_ref=dst, send_sem=send_sems.at[k], recv_sem=recv_sems.at[k],
            device_id=peer, device_id_type=MESH,
        )
        into = pltpu.make_async_remote_copy(
            src_ref=incoming, dst_ref=incoming, send_sem=send_sems.at[k], recv_sem=recv_sems.at[k],
            device_id=peer, device_id_type=MESH,
        )
        out.start()
        started.append(out)
        return into.wait_recv

    colour = m4(x + 2 * y)

    def quarter(zo, q, part=None):
        if part is None:
            return wd.at[m8(zo), pl.ds(pl.multiple_of(m4(q) * 32, 32), 32)]
        return wd.at[m8(zo), pl.ds(pl.multiple_of(m4(q) * 32 + 16 * part, 16), 16)]

    def ring(view):
        def start(step):
            if step < 4:
                a = remote(view(z - step + 1), view(z - step + 1), zp, view(z - step))
                b = remote(view(z + step - 1), view(z + step - 1), zm, view(z + step))
            else:
                a = remote(view(z - 3, 0), view(z - 3, 0), zp, view(z - 4, 0))
                b = remote(view(z + 3, 1), view(z + 3, 1), zm, view(z + 4, 1))
            return a, b

        return start

    local[0].wait()
    local[1].wait()
    down_ring = ring(lambda zo, part=None: quarter(zo, colour, part))
    waits = down_ring(1)
    local[2].wait()
    tokens_in = remote(tk, pt, partner, pt)
    sides = []

    def share(zo):
        own = quarter(zo, colour)
        sides.append(remote(own, own, xp, quarter(zo, colour - 1)))
        sides.append(remote(own, own, xm, quarter(zo, colour + 1)))
        for peer, part in ((yp, 0), (ym, 1)):
            half = quarter(zo, colour, part)
            sides.append(remote(half, half, peer, quarter(zo, colour + 2, part)))

    local[3].wait()
    for h in range(4):
        wup[dp, :, NOPE * h : NOPE * (h + 1)] = wqs[:, 192 * h : 192 * h + NOPE]
    wup[dp, :, Q_WIDTH : Q_WIDTH + R_WIDTH] = jnp.concatenate(
        [wqs[:, 192 * h + NOPE : 192 * (h + 1)] for h in range(4)], axis=1
    )
    for copy in local[6:10]:
        copy.wait()
    own_tab = tab[y]
    kr = dot(tk[...], wrot[...])
    kr_swap = jnp.concatenate([kr[:, 32:], kr[:, :32]], axis=1)
    kr = (kr * own_tab[:, :64] + kr_swap * own_tab[:, 64:]).astype(BF16)
    packed = jnp.concatenate([kr[:128], kr[128:]], axis=1)
    for t in range(4):
        kvb[sp, BLOCK:KV_ROWS, 128 * t : 128 * (t + 1)] = packed[32 * t : 32 * (t + 1)]

    for step in range(1, 5):
        for wait in waits:
            wait()
        if step < 4:
            waits = down_ring(step + 1)
            share(z - step)
            share(z + step)
        else:
            share(z + 4)
        if step == 1:
            tokens_in()
            for zo in range(8):
                columns = pl.ds(pl.multiple_of(256 * zo + 128 * c, 128), 128)
                lhs[0:256, 128 * zo : 128 * (zo + 1)] = tk[:, columns]
                lhs[256:512, 128 * zo : 128 * (zo + 1)] = pt[:, columns]

    local[4].wait()

    def up_block(zo, part=None, core=c):
        if part is None:
            return wup.at[m8(zo) * 2 + core]
        return wup.at[m8(zo) * 2 + core, pl.ds(16 * part, 16)]

    up_ring = ring(up_block)
    handed = []

    def hand_up(zo):
        handed.append(remote(up_block(zo), up_block(zo), partner, up_block(zo, core=1 - c)))

    up_waits = up_ring(1)
    hand_up(z)

    for wait in sides:
        wait()
    weights = wd[...].reshape(1024, 1024)
    part_send[...] = dot(lhs[256:512], weights)
    partial_in = remote(part_send, part_recv, partner, part_recv)
    own = dot(lhs[0:256], weights)
    partial_in()
    own = own + part_recv[...]

    def norm(v, gain):
        return v * lax.rsqrt(jnp.mean(v * v, axis=-1, keepdims=True) + EPSILON) * gain

    kvb[sp, 0:BLOCK, :] = norm(own[:, RANK:], kv_gain[...]).astype(BF16)
    qb[y] = norm(own[:, :RANK], q_gain[...]).astype(BF16)

    mid_a, mid_b = A_ROWS // 2, A_ROWS + (KV_ROWS - A_ROWS) // 2

    def rows_of(oy, ox, lo, hi):
        return kvb.at[m4(oy) * 4 + m4(ox), pl.ds(lo, hi - lo)]

    def a_piece(oy, ox, part=None):
        lo, hi = ((0, A_ROWS), (0, mid_a), (mid_a, A_ROWS))[0 if part is None else part + 1]
        return rows_of(oy, ox, lo, hi)

    def b_piece(oy, ox, part=None):
        lo, hi = ((A_ROWS, KV_ROWS), (A_ROWS, mid_b), (mid_b, KV_ROWS))[0 if part is None else part + 1]
        return rows_of(oy, ox, lo, hi)

    def q_piece(oy, ox, part=None):
        if part is None:
            return qb.at[m4(oy)]
        return qb.at[m4(oy), pl.ds(128 * part, 128)]

    def x_first(piece, oy):
        return (
            remote(piece(oy, x), piece(oy, x), xp, piece(oy, x - 1)),
            remote(piece(oy, x), piece(oy, x), xm, piece(oy, x + 1)),
        )

    def x_second(piece, oy):
        return (
            remote(piece(oy, x - 1, 0), piece(oy, x - 1, 0), xp, piece(oy, x - 2, 0)),
            remote(piece(oy, x + 1, 1), piece(oy, x + 1, 1), xm, piece(oy, x + 2, 1)),
        )

    def y_first(piece, ox):
        return (
            remote(piece(y, ox), piece(y, ox), yp, piece(y - 1, ox)),
            remote(piece(y, ox), piece(y, ox), ym, piece(y + 1, ox)),
        )

    def y_second(piece, ox):
        return (
            remote(piece(y - 1, ox, 0), piece(y - 1, ox, 0), yp, piece(y - 2, ox, 0)),
            remote(piece(y + 1, ox, 1), piece(y + 1, ox, 1), ym, piece(y + 2, ox, 1)),
        )

    def wait_all(waits):
        for wait in waits:
            wait()

    def up_step(step):
        wait_all(up_waits)
        nxt = up_ring(step + 1) if step < 4 else ()
        if step < 4:
            hand_up(z - step)
            hand_up(z + step)
        else:
            hand_up(z + 4)
        return nxt

    ax1 = x_first(a_piece, y)
    by1 = y_first(b_piece, x)
    bx1 = {0: x_first(b_piece, y)}
    qy1 = y_first(q_piece, x)
    ay1 = {0: y_first(a_piece, x)}
    bx2, ay2 = {}, {}

    local[5].wait()

    def out_view(chunk, core=c):
        def view(zo, part=None):
            lo, size = (1024 * chunk, 1024) if part is None else (1024 * chunk + 512 * part, 512)
            return wo.at[pl.ds(lo, size), pl.ds(pl.multiple_of(m8(zo) * 256 + core * 128, 128), 128)]

        return view

    out_rings = [ring(out_view(chunk)) for chunk in range(2)]
    out_waits = [None, None]

    def hand_out(chunk, zo):
        mine, other = out_view(chunk)(zo), out_view(chunk, 1 - c)(zo)
        handed.append(remote(mine, mine, partner, other))

    def out_start():
        for chunk in range(2):
            out_waits[chunk] = out_rings[chunk](1)
            hand_out(chunk, z)

    def out_step(step):
        for chunk in range(2):
            wait_all(out_waits[chunk])
            if step < 4:
                out_waits[chunk] = out_rings[chunk](step + 1)
                hand_out(chunk, z - step)
                hand_out(chunk, z + step)
            else:
                hand_out(chunk, z + 4)

    wait_all(ax1)
    ax2 = x_second(a_piece, y)
    ay1[-1] = y_first(a_piece, x - 1)
    ay1[1] = y_first(a_piece, x + 1)
    wait_all(by1)
    by2 = y_second(b_piece, x)
    bx1[-1] = x_first(b_piece, y - 1)
    bx1[1] = x_first(b_piece, y + 1)
    wait_all(bx1[0])
    bx2[0] = x_second(b_piece, y)
    up_waits = up_step(1)
    wait_all(qy1)
    qy2 = y_second(q_piece, x)
    wait_all(ax2)
    ay1[2] = y_first(a_piece, x + 2)
    wait_all(ay1[0])
    ay2[0] = y_second(a_piece, x)
    up_waits = up_step(2)
    wait_all(by2)
    bx1[2] = x_first(b_piece, y + 2)
    wait_all(bx2[0])
    up_waits = up_step(3)
    up_step(4)
    out_start()
    wait_all(handed[:8])
    del handed[:8]
    wait_all(ay1[-1])
    ay2[-1] = y_second(a_piece, x - 1)
    wait_all(ay1[1])
    ay2[1] = y_second(a_piece, x + 1)

    lane = lax.broadcasted_iota(jnp.int32, (256, 256), 1)
    first_half = lax.rem(lane, 64) < 32
    low = lax.rem(lax.broadcasted_iota(jnp.int32, (256, 128), 1), 128) < 64

    def expand_queries(i):
        up = dot(qb[i], wup[:, :, 0 : Q_WIDTH + R_WIDTH].reshape(RANK, Q_WIDTH + R_WIDTH))
        table = tab[i]
        cosine = jnp.concatenate([table[:, :64]] * 4, axis=1)
        sine = jnp.concatenate([table[:, 64:]] * 4, axis=1)
        u = up[:, Q_WIDTH:]
        swapped = jnp.where(first_half, pltpu.roll(u, R_WIDTH - 32, 1), pltpu.roll(u, 32, 1))
        turned = u * cosine + swapped * sine
        for h in range(4):
            qcat[h, i, :, 0:NOPE] = up[:, NOPE * h : NOPE * (h + 1)].astype(BF16)
            pair = turned[:, 128 * (h // 2) : 128 * (h // 2 + 1)]
            keep = low if h % 2 == 0 else jnp.logical_not(low)
            qcat[h, i, :, NOPE:256] = jnp.where(keep, pair, 0.0).astype(BF16)

    def expand_keys(o):
        up = dot(kvb[o, 0:BLOCK, :], wup[:, :, Q_WIDTH + R_WIDTH :].reshape(RANK, 1024)).astype(BF16)
        for h in range(4):
            kcat[h, o, :, 0:NOPE] = up[:, 256 * h : 256 * h + NOPE]
            vbuf[h, o] = up[:, 256 * h + NOPE : 256 * (h + 1)]
        for t in range(4):
            pair = kvb[o, BLOCK:KV_ROWS, 128 * t : 128 * (t + 1)].astype(F32)
            turned = pltpu.roll(pair, 64, 1)
            first = jnp.where(low[:32], pair, turned).astype(BF16)
            second = jnp.where(low[:32], turned, pair).astype(BF16)
            for h in range(4):
                kcat[h, o, 32 * t : 32 * (t + 1), NOPE:256] = first
                kcat[h, o, 128 + 32 * t : 128 + 32 * (t + 1), NOPE:256] = second

    def expand_row(r):
        def step(j, carry):
            expand_keys(r * 4 + j)
            return carry

        lax.fori_loop(0, 4, step, 0)

    def attend(i, r, masked):
        def pair(g, carry):
            for h in (2 * g, 2 * g + 1):
                k = kcat[h, pl.ds(4 * r, 4)].reshape(1024, 256)
                v = vbuf[h, pl.ds(4 * r, 4)].reshape(1024, VDIM)
                s = lax.dot_general(qcat[h, i], k, (((1,), (1,)), ((), ())), preferred_element_type=F32)
                s = s * SCALE
                if masked:
                    q_pos = lax.broadcasted_iota(jnp.int32, (256, 1024), 0) + x * 256
                    k_pos = lax.broadcasted_iota(jnp.int32, (256, 1024), 1)
                    s = jnp.where(k_pos <= q_pos, s, -jnp.inf)
                old = mbuf[h, i]
                top = jnp.maximum(old, jnp.max(s, axis=-1, keepdims=True))
                p = jnp.exp2(s - top[:, :1])
                alpha = jnp.exp2(old - top)
                mbuf[h, i] = top
                lbuf[h, i] = lbuf[h, i] * alpha + jnp.sum(p, axis=-1, keepdims=True)
                acc[h, i] = acc[h, i] * alpha + dot(p.astype(BF16), v)
            return carry

        lax.fori_loop(0, 2, pair, 0)

    def attend_row(r):
        attend(r, r, True)

        def step(i, carry):
            attend(i, r, False)
            return carry

        lax.fori_loop(r + 1, 4, step, 0)

    acc[...] = jnp.zeros_like(acc)
    lbuf[...] = jnp.zeros_like(lbuf)
    mbuf[...] = jnp.full_like(mbuf, -jnp.inf)

    wait_all(qy2)

    def expand_query_block(i, carry):
        expand_queries(i)
        return carry

    lax.fori_loop(0, 4, expand_query_block, 0)
    expand_row(y)
    wait_all(bx1[1])
    bx2[1] = x_second(b_piece, y + 1)
    wait_all(bx1[-1])
    bx2[-1] = x_second(b_piece, y - 1)
    wait_all(ay1[2])
    ay2[2] = y_second(a_piece, x + 2)
    attend_row(y)
    out_step(1)
    wait_all(bx1[2])
    bx2[2] = x_second(b_piece, y + 2)
    wait_all(bx2[1])
    expand_row(m4(y + 1))
    attend_row(m4(y + 1))
    out_step(2)
    wait_all(bx2[-1])
    expand_row(m4(y - 1))
    attend_row(m4(y - 1))
    out_step(3)
    for delta in (0, -1, 1, 2):
        wait_all(ay2[delta])
    wait_all(bx2[2])
    expand_row(m4(y + 2))
    attend_row(m4(y + 2))

    def finish(i, carry):
        for h in range(4):
            osend[i, :, VDIM * h : VDIM * (h + 1)] = (acc[h, i] / lbuf[h, i]).astype(BF16)
        return carry

    lax.fori_loop(0, 4, finish, 0)
    back = []
    for delta in (2, 1, 3):
        back.append(
            remote(osend.at[m4(y + delta)], orecv.at[y], plane(y + delta, x), orecv.at[m4(y - delta)])
        )
    orecv[y] = osend[y]
    out_step(4)
    wait_all(handed)
    wait_all(back)

    def project(j, total):
        return total + dot(orecv[j], wo[pl.ds(pl.multiple_of(512 * j, 512), 512), :])

    total = jnp.zeros((BLOCK, D), F32)
    for j in range(4):
        total = project(j, total)
    out_ref[...] = norm(total, out_gain[...]).astype(BF16)
    for copy in started:
        copy.wait_send()


N_COPIES = 176


def body(tokens, w_qdown, w_kvdown, w_rotary, q_gain, kv_gain, w_qup, w_kvup, w_out, out_gain):
    table = jnp.asarray(turn_table())
    any_spec = pl.BlockSpec(memory_space=pl.ANY)
    vmem_spec = pl.BlockSpec(memory_space=pltpu.VMEM)
    call = pl.pallas_call(
        kernel,
        out_shape=jax.ShapeDtypeStruct((BLOCK, D), BF16),
        in_specs=[any_spec, any_spec, any_spec, vmem_spec, vmem_spec, vmem_spec]
        + [any_spec, any_spec, any_spec, vmem_spec, any_spec],
        out_specs=vmem_spec,
        scratch_shapes=[
            pltpu.VMEM((BLOCK, D), BF16),
            pltpu.VMEM((BLOCK, D), BF16),
            pltpu.VMEM((2 * BLOCK, 1024), BF16),
            pltpu.VMEM((8, 128, 1024), BF16),
            pltpu.VMEM((BLOCK, 1024), F32),
            pltpu.VMEM((BLOCK, 1024), F32),
            pltpu.VMEM((16, KV_ROWS, RANK), BF16),
            pltpu.VMEM((4, BLOCK, RANK), BF16),
            pltpu.VMEM((32, 768), BF16),
            pltpu.VMEM((16, 32, UP_WIDTH), BF16),
            pltpu.VMEM((D, D), BF16),
            pltpu.VMEM((4, BLOCK, 128), F32),
            pltpu.VMEM((4, 16, BLOCK, 256), BF16),
            pltpu.VMEM((4, 16, BLOCK, VDIM), BF16),
            pltpu.VMEM((4, 4, BLOCK, 256), BF16),
            pltpu.VMEM((4, 4, BLOCK, VDIM), F32),
            pltpu.VMEM((4, 4, BLOCK, 128), F32),
            pltpu.VMEM((4, 4, BLOCK, 128), F32),
            pltpu.VMEM((4, BLOCK, 512), BF16),
            pltpu.VMEM((4, BLOCK, 512), BF16),
            pltpu.SemaphoreType.DMA((N_COPIES,)),
            pltpu.SemaphoreType.DMA((N_COPIES,)),
            pltpu.SemaphoreType.DMA((10,)),
        ],
        compiler_params=pltpu.CompilerParams(
            collective_id=0, has_side_effects=True, vmem_limit_bytes=63 * 1024 * 1024
        ),
        name="latent_attention",
    )
    mixed = call(
        tokens[0], w_qdown, w_kvdown, w_rotary, q_gain[None], kv_gain[None],
        w_qup, w_kvup, w_out, out_gain[None], table,
    )
    return mixed[None]


def solution(mesh):
    in_specs = (
        P("dp", "sp", None),
        P("dp", None),
        P("dp", None),
        P(),
        P(),
        P(),
        P("dp", None),
        P("dp", None),
        P(None, "dp"),
        P(),
    )
    out_specs = P("dp", "sp", None)
    return jax.shard_map(body, mesh=mesh, in_specs=in_specs, out_specs=out_specs, check_vma=False)
```

time: 236 us -> 131 us (0.56)
  the two profiles are of different devices: /device:TPU:32 before, /device:TPU:1 now
where the time goes in v1:
time: 131 us
  Pallas kernels  127 us (97%)
  local copies, waits for them, and re-layouts  4.26 us (3%)
    pallas_call x1, Pallas kernels, body(): call(tokens[0], w_qdown, w_kvdown, w_rotary, q_gain[None], kv_gain[None],...  127 us
    unnamed x2, local copies, waits for them, and re-layouts  4.26 us

profile of v1, /device:TPU:1, one launch (start us, length us, event | category | flops | bytes accessed | tf_op | source)
XLA Modules:
  0.0 130.9 jit_solution(579644247237832019)
XLA Ops:
  0.0 2.0 %copy.12.wrot = bf16[2048,64]{1,0:T(8,128)(2,1)} copy(bf16[2048,64]{0,1:T(8,128)(2,1)} %param.14) | data formatting | bytes 524288 | tf_op args[3]
  2.0 126.6 %latent_attention.1 = bf16[256,2048]{1,0:T(8,128)(2,1)} custom-call(bf16[256,2048]{1,0:T(8,128)(2,1)} %bitcast.6, bf16[128,512]{1,0:T(8,128)(2,1)} %wq_hbm.1, bf16[128,512]{1,0:T(8,128)(2,1)} %wkv_hbm.1, bf16[2048,64]{1,0:T(8,128)(2,1)} %copy.12.wrot, f32[1,512]{1,0:T(1,128)} %bitcast.8, f32[1,512]{1,0:T(1,128)} %bitcast.9, bf16[32,3072]{1,0:T(8,128)(2,1)} %wqup_hbm.1, ...), custom_call_target="tpu_custom_call" | custom-call | tf_op jit(solution)/shard_map/latent_attention/pallas_call | solution.py:518
  128.6 2.3 %copy.14 = bf16[1,256,2048]{2,1,0:T(8,128)(2,1)} copy(bf16[1,256,2048]{2,1,0:T(8,128)(2,1)} %bitcast.5) | data formatting | bytes 2097152

commit v2 on v0

v2 whole, which is shorter than its diff:
```python
import functools

import jax
import jax.numpy as jnp
import numpy as np
from jax import lax
from jax.experimental import pallas as pl
from jax.experimental.pallas import tpu as pltpu
from jax.sharding import PartitionSpec as P

HEADS = 16
NOPE = 128
ROPE = 64
VDIM = 128
D = 2048
RANK = 512
LENGTH = 4096
BLOCK = 256
EPSILON = 1e-06
THETA = 10000.0
LOG2E = 1.4426950408889634
SCALE = (NOPE + ROPE) ** (-0.5) * LOG2E
MESH = pl.DeviceIdType.MESH
BF16 = jnp.bfloat16
F32 = jnp.float32
Q_WIDTH = 4 * NOPE
R_WIDTH = 4 * ROPE
UP_WIDTH = Q_WIDTH + R_WIDTH + 4 * (NOPE + VDIM)
A_ROWS = 96
KV_ROWS = BLOCK + 32


def turn_table():
    positions = np.arange(LENGTH).astype(np.float32)
    freqs = np.float32(THETA) ** (-np.arange(0, ROPE, 2).astype(np.float32) / np.float32(ROPE))
    angles = positions[:, None] * freqs[None, :].astype(np.float32)
    cosine, sine = np.cos(angles), np.sin(angles)
    return np.concatenate([cosine, cosine, -sine, sine], axis=1).astype(np.float32)


def dot(a, b):
    return jnp.dot(a, b, preferred_element_type=F32)


class Move:
    def __init__(self, sems, src, dst, peer, incoming):
        def make(a, b):
            return pltpu.make_async_remote_copy(
                src_ref=a, dst_ref=b, send_sem=sems[0], recv_sem=sems[1], device_id=peer, device_id_type=MESH
            )

        self.out, self.into = make(src, dst), make(incoming, incoming)

    def start(self):
        self.out.start()

    def wait(self):
        self.into.wait_recv()

    def finish(self):
        self.out.wait_send()


def start_all(moves):
    for move in moves:
        move.start()


def wait_all(moves):
    for move in moves:
        move.wait()


def norm(v, gain):
    return v * lax.rsqrt(jnp.mean(v * v, axis=-1, keepdims=True) + EPSILON) * gain


def kernel(
    tok_hbm, wq_hbm, wkv_hbm, wrot_hbm, q_gain, kv_gain, wqup_hbm, wkvup_hbm, wout_hbm, out_gain, tab_hbm,
    out_ref,
    tk, pt, lhs, wd, part_send, part_recv, kvb, qb, wqs, wup, wo, wrot, tab, kcat, vbuf, qcat, acc, mbuf,
    osend, orecv, send_sems, recv_sems, local_sems,
):
    sp, dp = lax.axis_index("sp"), lax.axis_index("dp")
    y, x = lax.div(sp, 4), lax.rem(sp, 4)
    z, c = lax.div(dp, 2), lax.rem(dp, 2)

    def m4(v):
        return lax.rem(v + 8, 4)

    def m8(v):
        return lax.rem(v + 16, 8)

    def plane(yy, xx):
        return (m4(yy) * 4 + m4(xx), dp)

    def along(zz):
        return (sp, m8(zz) * 2 + c)

    partner = (sp, z * 2 + (1 - c))
    xp, xm, yp, ym = plane(y, x + 1), plane(y, x - 1), plane(y + 1, x), plane(y - 1, x)
    zp, zm = along(z + 1), along(z - 1)

    local = [
        pltpu.make_async_copy(wkv_hbm, wd.at[z, :, pl.ds(0, RANK)], local_sems.at[0]),
        pltpu.make_async_copy(wq_hbm, wd.at[z, :, pl.ds(RANK, RANK)], local_sems.at[1]),
        pltpu.make_async_copy(tok_hbm, tk, local_sems.at[2]),
        pltpu.make_async_copy(
            wqup_hbm.at[:, pl.ds(pl.multiple_of(y * 768, 128), 768)], wqs, local_sems.at[3]
        ),
        pltpu.make_async_copy(
            wkvup_hbm.at[:, pl.ds(pl.multiple_of(y * 1024, 128), 1024)],
            wup.at[dp, :, pl.ds(Q_WIDTH + R_WIDTH, 1024)],
            local_sems.at[4],
        ),
        pltpu.make_async_copy(
            wout_hbm, wo.at[:, pl.ds(pl.multiple_of(dp * 128, 128), 128)], local_sems.at[5]
        ),
        pltpu.make_async_copy(wrot_hbm, wrot, local_sems.at[6]),
    ]
    for i in range(4):
        local.append(
            pltpu.make_async_copy(
                tab_hbm.at[pl.ds(pl.multiple_of(i * 1024 + x * 256, 256), 256)], tab.at[i], local_sems.at[7 + i]
            )
        )
    for copy in local:
        copy.start()

    moves = []

    def move(src, dst, peer, incoming):
        k = len(moves)
        moves.append(Move((send_sems.at[k], recv_sems.at[k]), src, dst, peer, incoming))
        return moves[-1]

    def ring(view):
        steps = {}
        for s in range(1, 4):
            up, down = view(z - s + 1), view(z + s - 1)
            steps[s] = (move(up, up, zp, view(z - s)), move(down, down, zm, view(z + s)))
        up, down = view(z - 3, 0), view(z + 3, 1)
        steps[4] = (move(up, up, zp, view(z - 4, 0)), move(down, down, zm, view(z + 4, 1)))
        return steps

    colour = m4(x + 2 * y)

    def quarter(ch, zo, q, part=None):
        columns = pl.ds(RANK * ch, RANK)
        if part is None:
            return wd.at[m8(zo), pl.ds(pl.multiple_of(m4(q) * 32, 32), 32), columns]
        return wd.at[m8(zo), pl.ds(pl.multiple_of(m4(q) * 32 + 16 * part, 16), 16), columns]

    def sides_of(ch, zo):
        own = quarter(ch, zo, colour)
        first, second = quarter(ch, zo, colour, 0), quarter(ch, zo, colour, 1)
        return (
            move(own, own, xp, quarter(ch, zo, colour - 1)),
            move(own, own, xm, quarter(ch, zo, colour + 1)),
            move(first, first, yp, quarter(ch, zo, colour + 2, 0)),
            move(second, second, ym, quarter(ch, zo, colour + 2, 1)),
        )

    down = [ring(functools.partial(lambda ch, zo, part=None: quarter(ch, zo, colour, part), ch)) for ch in range(2)]
    sides = [{d: sides_of(ch, z + d) for d in (-1, 1, -2, 2, -3, 3, 4)} for ch in range(2)]
    tokens_over = move(tk, pt, partner, pt)
    partial_over = [move(part_send.at[ch], part_recv.at[ch], partner, part_recv.at[ch]) for ch in range(2)]

    def up_block(zo, part=None, core=c):
        if part is None:
            return wup.at[m8(zo) * 2 + core]
        return wup.at[m8(zo) * 2 + core, pl.ds(16 * part, 16)]

    up = ring(up_block)
    up_hand = {
        d: move(up_block(z + d), up_block(z + d), partner, up_block(z + d, core=1 - c))
        for d in (0, -1, 1, -2, 2, -3, 3, 4)
    }

    def out_view(chunk, zo, part=None):
        lo, size = (512 * chunk, 512) if part is None else (512 * chunk + 256 * part, 256)
        return wo.at[pl.ds(lo, size), pl.ds(pl.multiple_of(m8(zo) * 256 + c * 128, 128), 128)]

    def out_column(zo, core):
        return wo.at[:, pl.ds(pl.multiple_of(m8(zo) * 256 + core * 128, 128), 128)]

    out = [ring(functools.partial(out_view, chunk)) for chunk in range(4)]
    out_hand = {
        d: move(out_column(z + d, c), out_column(z + d, c), partner, out_column(z + d, 1 - c))
        for d in (0, -1, 1, -2, 2, -3, 3, 4)
    }

    def hand(hands, step):
        for d in (-step, step) if step < 4 else (4,):
            hands[d].start()

    def out_visit(step, chunk):
        wait_all(out[chunk][step])
        if step < 4:
            start_all(out[chunk][step + 1])
        if chunk == 3:
            hand(out_hand, step)

    mid_a, mid_b = A_ROWS // 2, A_ROWS + (KV_ROWS - A_ROWS) // 2

    def rows_of(spans, oy, ox, part=None):
        lo, hi = spans[0 if part is None else part + 1]
        return kvb.at[m4(oy) * 4 + m4(ox), pl.ds(lo, hi - lo)]

    a_piece = functools.partial(rows_of, ((0, A_ROWS), (0, mid_a), (mid_a, A_ROWS)))
    b_piece = functools.partial(rows_of, ((A_ROWS, KV_ROWS), (A_ROWS, mid_b), (mid_b, KV_ROWS)))

    def q_piece(oy, ox, part=None):
        if part is None:
            return qb.at[m4(oy)]
        return qb.at[m4(oy), pl.ds(128 * part, 128)]

    def x_first(piece, oy):
        own = piece(oy, x)
        return move(own, own, xp, piece(oy, x - 1)), move(own, own, xm, piece(oy, x + 1))

    def x_second(piece, oy):
        left, right = piece(oy, x - 1, 0), piece(oy, x + 1, 1)
        return move(left, left, xp, piece(oy, x - 2, 0)), move(right, right, xm, piece(oy, x + 2, 1))

    def y_first(piece, ox):
        own = piece(y, ox)
        return move(own, own, yp, piece(y - 1, ox)), move(own, own, ym, piece(y + 1, ox))

    def y_second(piece, ox):
        under, over = piece(y - 1, ox, 0), piece(y + 1, ox, 1)
        return move(under, under, yp, piece(y - 2, ox, 0)), move(over, over, ym, piece(y + 2, ox, 1))

    ax1, ax2 = x_first(a_piece, y), x_second(a_piece, y)
    ay1 = {d: y_first(a_piece, x + d) for d in (0, -1, 1, 2)}
    ay2 = {d: y_second(a_piece, x + d) for d in (0, -1, 1, 2)}
    by1, by2 = y_first(b_piece, x), y_second(b_piece, x)
    bx1 = {d: x_first(b_piece, y + d) for d in (0, -1, 1, 2)}
    bx2 = {d: x_second(b_piece, y + d) for d in (0, -1, 1, 2)}
    qy1, qy2 = y_first(q_piece, x), y_second(q_piece, x)
    back = {
        d: move(osend.at[m4(y + d)], orecv.at[y], plane(y + d, x), orecv.at[m4(y - d)]) for d in (2, 1, 3)
    }

    barrier = pltpu.get_barrier_semaphore()
    for peer in (xp, xm, yp, ym, plane(y + 2, x), zp, zm, partner):
        pl.semaphore_signal(barrier, inc=1, device_id=peer, device_id_type=MESH)
    pl.semaphore_wait(barrier, 8)

    local[0].wait()
    start_all(down[0][1])
    local[1].wait()
    start_all(down[1][1])
    local[2].wait()
    tokens_over.start()

    local[3].wait()
    for h in range(4):
        wup[dp, :, NOPE * h : NOPE * (h + 1)] = wqs[:, 192 * h : 192 * h + NOPE]
    wup[dp, :, Q_WIDTH : Q_WIDTH + R_WIDTH] = jnp.concatenate(
        [wqs[:, 192 * h + NOPE : 192 * (h + 1)] for h in range(4)], axis=1
    )
    local[4].wait()
    start_all(up[1])
    up_hand[0].start()

    for copy in local[6:11]:
        copy.wait()
    own_tab = tab[y]
    kr = lax.dot_general(tk[...], wrot[...], (((1,), (1,)), ((), ())), preferred_element_type=F32)
    kr_swap = jnp.concatenate([kr[:, 32:], kr[:, :32]], axis=1)
    kr = (kr * own_tab[:, :64] + kr_swap * own_tab[:, 64:]).astype(BF16)
    packed = jnp.concatenate([kr[:128], kr[128:]], axis=1)
    for t in range(4):
        kvb[sp, BLOCK:KV_ROWS, 128 * t : 128 * (t + 1)] = packed[32 * t : 32 * (t + 1)]

    for step in range(1, 5):
        for ch in range(2):
            wait_all(down[ch][step])
            if step < 4:
                start_all(down[ch][step + 1])
            for d in (-step, step) if step < 4 else (4,):
                start_all(sides[ch][d])
        if step == 1:
            tokens_over.wait()
            for zo in range(8):
                columns = pl.ds(pl.multiple_of(256 * zo + 128 * c, 128), 128)
                lhs[0:256, 128 * zo : 128 * (zo + 1)] = tk[:, columns]
                lhs[256:512, 128 * zo : 128 * (zo + 1)] = pt[:, columns]
        else:
            wait_all(up[step - 1])
            start_all(up[step])
            hand(up_hand, step - 1)
        if step == 2:
            acc[...] = jnp.zeros_like(acc)
            mbuf[...] = jnp.full_like(mbuf, -jnp.inf)
        if step == 3:
            for h in range(4):
                vbuf[h, :, :, VDIM:256] = jnp.ones((16, BLOCK, 256 - VDIM), BF16)

    local[5].wait()
    for chunk in range(4):
        start_all(out[chunk][1])

    def down_project(ch):
        for d in (-1, 1, -2, 2, -3, 3, 4):
            wait_all(sides[ch][d])
        weights = wd[:, :, RANK * ch : RANK * (ch + 1)].reshape(1024, RANK)
        part_send[ch] = dot(lhs[256:512], weights)
        partial_over[ch].start()
        own = dot(lhs[0:256], weights)
        partial_over[ch].wait()
        return own + part_recv[ch]

    kvb[sp, 0:BLOCK, :] = norm(down_project(0), kv_gain[...]).astype(BF16)
    start_all(ax1 + bx1[0] + by1 + ay1[0])
    qb[y] = norm(down_project(1), q_gain[...]).astype(BF16)
    start_all(qy1)
    wait_all(up[4])
    hand(up_hand, 4)

    def expand_queries(i):
        rows = dot(qb[i], wup[:, :, 0 : Q_WIDTH + R_WIDTH].reshape(RANK, Q_WIDTH + R_WIDTH))
        first_half = lax.rem(lax.broadcasted_iota(jnp.int32, (BLOCK, R_WIDTH), 1), 64) < 32
        low = lax.broadcasted_iota(jnp.int32, (BLOCK, 128), 1) < 64
        table = tab[i]
        cosine = jnp.concatenate([table[:, :64]] * 4, axis=1)
        sine = jnp.concatenate([table[:, 64:]] * 4, axis=1)
        u = rows[:, Q_WIDTH:]
        swapped = jnp.where(first_half, pltpu.roll(u, R_WIDTH - 32, 1), pltpu.roll(u, 32, 1))
        turned = u * cosine + swapped * sine
        for h in range(4):
            qcat[h, i, :, 0:NOPE] = rows[:, NOPE * h : NOPE * (h + 1)].astype(BF16)
            pair = turned[:, 128 * (h // 2) : 128 * (h // 2 + 1)]
            keep = low if h % 2 == 0 else jnp.logical_not(low)
            qcat[h, i, :, NOPE:256] = jnp.where(keep, pair, 0.0).astype(BF16)

    def expand_keys(oy, ox):
        o = m4(oy) * 4 + m4(ox)
        rows = dot(kvb[o, 0:BLOCK, :], wup[:, :, Q_WIDTH + R_WIDTH :].reshape(RANK, 1024)).astype(BF16)
        low = lax.broadcasted_iota(jnp.int32, (32, 128), 1) < 64
        for h in range(4):
            kcat[h, o, :, 0:NOPE] = rows[:, 256 * h : 256 * h + NOPE]
            vbuf[h, o, :, 0:VDIM] = rows[:, 256 * h + NOPE : 256 * (h + 1)]
        for t in range(4):
            pair = kvb[o, BLOCK:KV_ROWS, 128 * t : 128 * (t + 1)].astype(F32)
            turned = pltpu.roll(pair, 64, 1)
            first = jnp.where(low, pair, turned).astype(BF16)
            second = jnp.where(low, turned, pair).astype(BF16)
            for h in range(4):
                kcat[h, o, 32 * t : 32 * (t + 1), NOPE:256] = first
                kcat[h, o, 128 + 32 * t : 128 + 32 * (t + 1), NOPE:256] = second

    def expand_many(which):
        dy, dxs = which

        def step(j, carry):
            expand_keys(y + dy, x + dxs[0] + j * (dxs[-1] - dxs[0]))
            return carry

        lax.fori_loop(0, len(dxs), step, 0)

    wait_all(ax1)
    start_all(ax2 + ay1[-1] + ay1[1])
    wait_all(bx1[0])
    start_all(bx2[0])
    wait_all(by1)
    start_all(by2 + bx1[1] + bx1[-1])
    wait_all(up_hand.values())
    expand_many((0, (0,)))
    expand_queries(y)
    wait_all(ay1[0])
    start_all(ay2[0])
    wait_all(ax2)
    start_all(ay1[2])
    out_visit(1, 0)
    expand_many((0, (-1, 1)))
    wait_all(qy1)
    start_all(qy2)
    out_visit(1, 1)

    def near_queries(j, carry):
        expand_queries(m4(y - 1 + 2 * j))
        return carry

    lax.fori_loop(0, 2, near_queries, 0)
    wait_all(by2)
    start_all(bx1[2])
    wait_all(bx2[0])
    expand_many((0, (2,)))
    out_visit(1, 2)

    def attend(i, r, masked):
        def scores_of(h):
            k = kcat[h, pl.ds(4 * r, 4)].reshape(1024, 256)
            return lax.dot_general(qcat[h, i], k, (((1,), (1,)), ((), ())), preferred_element_type=F32)

        def take(h, s):
            if masked:
                q_pos = lax.broadcasted_iota(jnp.int32, (256, 1024), 0) + x * 256
                k_pos = lax.broadcasted_iota(jnp.int32, (256, 1024), 1)
                s = jnp.where(k_pos <= q_pos, s, -jnp.inf)
            old = mbuf[h, i]
            top = jnp.maximum(old, jnp.max(s, axis=-1, keepdims=True) * SCALE)
            p = jnp.exp2(s * SCALE - top[:, :1]).astype(BF16)
            alpha = jnp.exp2(old - top)
            mbuf[h, i] = top
            v = vbuf[h, pl.ds(4 * r, 4)].reshape(1024, 256)
            acc[h, i] = acc[h, i] * jnp.concatenate([alpha, alpha], axis=1) + dot(p, v)

        ahead = scores_of(0)
        for h in range(4):
            s, ahead = ahead, scores_of(h + 1) if h < 3 else None
            take(h, s)

    def finish(i):
        for h in range(4):
            done = acc[h, i]
            osend[i, :, VDIM * h : VDIM * (h + 1)] = (done[:, :VDIM] / done[:, VDIM:]).astype(BF16)

    def at_1():
        wait_all(ay1[-1])
        start_all(ay2[-1])
        wait_all(ay1[1])
        start_all(ay2[1])

    def at_2():
        wait_all(bx1[1])
        start_all(bx2[1])
        wait_all(bx1[-1])
        start_all(bx2[-1])

    def at_3():
        wait_all(qy2)
        expand_queries(m4(y + 2))

    def at_4():
        wait_all(ay1[2])
        start_all(ay2[2])
        expand_many((1, (0,)))
        expand_many((1, (-1, 1)))
        wait_all(bx2[1])
        expand_many((1, (2,)))

    def at_6():
        wait_all(bx1[2])
        start_all(bx2[2])

    def at_8():
        expand_many((-1, (0,)))
        expand_many((-1, (-1, 1)))
        wait_all(bx2[-1])
        expand_many((-1, (2,)))

    def at_12():
        wait_all(ay2[0])
        expand_many((2, (0,)))
        wait_all(ay2[-1] + ay2[1])
        expand_many((2, (-1, 1)))
        wait_all(ay2[2] + bx2[2])
        expand_many((2, (2,)))

    events = {1: at_1, 2: at_2, 3: at_3, 4: at_4, 6: at_6, 8: at_8, 12: at_12}
    visits = {0: (1, 3), 1: (2, 0), 2: (2, 1), 3: (2, 2), 4: (2, 3), 6: (3, 0), 7: (3, 1), 8: (3, 2), 9: (3, 3)}

    def slot(v, done):
        rho, kappa = lax.div(v, 4), lax.rem(v, 4)
        swap = jnp.where(kappa == 2, 3, jnp.where(kappa == 3, 2, kappa))
        dr = jnp.where(rho == 2, 3, jnp.where(rho == 3, 2, rho))
        last = jnp.where(kappa == 0, 2, jnp.where(kappa == 2, 3, jnp.where(kappa == 3, 0, 1)))
        r, i = m4(y + dr), m4(y + jnp.where(rho == 3, last, swap))
        for at, event in events.items():
            pl.when(v == at)(event)
        pl.when(i == r)(lambda: attend(i, r, True))
        pl.when(i > r)(lambda: attend(i, r, False))
        active = i >= r
        for number, (step, chunk) in visits.items():
            pl.when(jnp.logical_and(active, done == number))(functools.partial(out_visit, step, chunk))
        pl.when(rho == 3)(lambda: finish(i))
        for at, d in ((12, 2), (13, 1), (14, 3)):
            pl.when(v == at)(back[d].start)
        return done + active.astype(jnp.int32)

    lax.fori_loop(0, 16, slot, jnp.int32(0))

    out_hand[0].start()
    for chunk in range(4):
        out_visit(4, chunk)
    wait_all(out_hand.values())

    def project(attended, j):
        return dot(attended, wo[pl.ds(pl.multiple_of(512 * j, 512), 512), :])

    total = project(osend[y], y)
    for d in (3, 1, 2):
        back[d].wait()
        total = total + project(orecv[m4(y - d)], m4(y - d))
    out_ref[...] = norm(total, out_gain[...]).astype(BF16)
    for each in moves:
        each.finish()


N_COPIES = 208


def body(tokens, w_qdown, w_kvdown, w_rotary, q_gain, kv_gain, w_qup, w_kvup, w_out, out_gain):
    table = jnp.asarray(turn_table())
    any_spec = pl.BlockSpec(memory_space=pl.ANY)
    vmem_spec = pl.BlockSpec(memory_space=pltpu.VMEM)
    call = pl.pallas_call(
        kernel,
        out_shape=jax.ShapeDtypeStruct((BLOCK, D), BF16),
        in_specs=[any_spec, any_spec, any_spec, any_spec, vmem_spec, vmem_spec]
        + [any_spec, any_spec, any_spec, vmem_spec, any_spec],
        out_specs=vmem_spec,
        scratch_shapes=[
            pltpu.VMEM((BLOCK, D), BF16),
            pltpu.VMEM((BLOCK, D), BF16),
            pltpu.VMEM((2 * BLOCK, 1024), BF16),
            pltpu.VMEM((8, 128, 1024), BF16),
            pltpu.VMEM((2, BLOCK, RANK), F32),
            pltpu.VMEM((2, BLOCK, RANK), F32),
            pltpu.VMEM((16, KV_ROWS, RANK), BF16),
            pltpu.VMEM((4, BLOCK, RANK), BF16),
            pltpu.VMEM((32, 768), BF16),
            pltpu.VMEM((16, 32, UP_WIDTH), BF16),
            pltpu.VMEM((D, D), BF16),
            pltpu.VMEM((ROPE, D), BF16),
            pltpu.VMEM((4, BLOCK, 128), F32),
            pltpu.VMEM((4, 16, BLOCK, 256), BF16),
            pltpu.VMEM((4, 16, BLOCK, 256), BF16),
            pltpu.VMEM((4, 4, BLOCK, 256), BF16),
            pltpu.VMEM((4, 4, BLOCK, 256), F32),
            pltpu.VMEM((4, 4, BLOCK, 128), F32),
            pltpu.VMEM((4, BLOCK, 512), BF16),
            pltpu.VMEM((4, BLOCK, 512), BF16),
            pltpu.SemaphoreType.DMA((N_COPIES,)),
            pltpu.SemaphoreType.DMA((N_COPIES,)),
            pltpu.SemaphoreType.DMA((11,)),
        ],
        compiler_params=pltpu.CompilerParams(
            collective_id=0, has_side_effects=True, vmem_limit_bytes=63 * 1024 * 1024
        ),
        name="latent_attention",
    )
    mixed = call(
        tokens[0], w_qdown, w_kvdown, w_rotary.T, q_gain[None], kv_gain[None],
        w_qup, w_kvup, w_out, out_gain[None], table,
    )
    return mixed[None]


def solution(mesh):
    in_specs = (
        P("dp", "sp", None),
        P("dp", None),
        P("dp", None),
        P(),
        P(),
        P(),
        P("dp", None),
        P("dp", None),
        P(None, "dp"),
        P(),
    )
    out_specs = P("dp", "sp", None)
    return jax.shard_map(body, mesh=mesh, in_specs=in_specs, out_specs=out_specs, check_vma=False)
```

time: 236 us -> 104 us (0.44)
  the two profiles are of different devices: /device:TPU:32 before, /device:TPU:1 now
where the time goes in v2:
time: 104 us
  Pallas kernels  102 us (98%)
  local copies, waits for them, and re-layouts  2.3 us (2%)
    pallas_call x1, Pallas kernels, body(): call(tokens[0], w_qdown, w_kvdown, w_rotary.T, q_gain[None], kv_gain[None...  102 us
    unnamed x1, local copies, waits for them, and re-layouts  2.3 us

profile of v2, /device:TPU:1, one launch (start us, length us, event | category | flops | bytes accessed | tf_op | source)
XLA Modules:
  0.0 104.0 jit_solution(3842349228093272883)
XLA Ops:
  0.0 101.7 %latent_attention.1 = bf16[256,2048]{1,0:T(8,128)(2,1)} custom-call(bf16[256,2048]{1,0:T(8,128)(2,1)} %bitcast.7, bf16[128,512]{1,0:T(8,128)(2,1)} %wq_hbm.1, bf16[128,512]{1,0:T(8,128)(2,1)} %wkv_hbm.1, bf16[64,2048]{1,0:T(8,128)(2,1)} %bitcast.8, f32[1,512]{1,0:T(1,128)} %bitcast.10, f32[1,512]{1,0:T(1,128)} %bitcast.11, bf16[32,3072]{1,0:T(8,128)(2,1)} %wqup_hbm.1, ...), custom_call_target="tpu_custom_call" | custom-call | tf_op jit(solution)/shard_map/latent_attention/pallas_call | solution.py:546
  101.7 2.3 %copy.13 = bf16[1,256,2048]{2,1,0:T(8,128)(2,1)} copy(bf16[1,256,2048]{2,1,0:T(8,128)(2,1)} %bitcast.6) | data formatting | bytes 2097152

commit v3 on v2

--- a/solution.py
+++ b/solution.py
@@ -27,6 +27,9 @@
 R_WIDTH = 4 * ROPE
 UP_WIDTH = Q_WIDTH + R_WIDTH + 4 * (NOPE + VDIM)
 A_ROWS = 96
+PLACE = {0: 0, -1: 1, 1: 2, 2: 3}
+KEY_BLOCKS = 4
+SUBS = 4 // KEY_BLOCKS
 KV_ROWS = BLOCK + 32
 
 
@@ -161,8 +164,11 @@
             move(second, second, ym, quarter(ch, zo, colour + 2, 1)),
         )
 
-    down = [ring(functools.partial(lambda ch, zo, part=None: quarter(ch, zo, colour, part), ch)) for ch in range(2)]
-    sides = [{d: sides_of(ch, z + d) for d in (-1, 1, -2, 2, -3, 3, 4)} for ch in range(2)]
+    near = (-1, 1, -2, 2, -3, 3, 4)
+    own_quarter = quarter(0, z, colour)
+    direct = {d: move(own_quarter, own_quarter, along(z + d), quarter(0, z - d, colour)) for d in near}
+    down = ring(lambda zo, part=None: quarter(1, zo, colour, part))
+    sides = [{d: sides_of(ch, z + d) for d in near} for ch in range(2)]
     tokens_over = move(tk, pt, partner, pt)
     partial_over = [move(part_send.at[ch], part_recv.at[ch], partner, part_recv.at[ch]) for ch in range(2)]
 
@@ -243,16 +249,17 @@
     }
 
     barrier = pltpu.get_barrier_semaphore()
-    for peer in (xp, xm, yp, ym, plane(y + 2, x), zp, zm, partner):
+    for peer in (xp, xm, yp, ym, plane(y + 2, x), partner) + tuple(along(z + d) for d in near):
         pl.semaphore_signal(barrier, inc=1, device_id=peer, device_id_type=MESH)
-    pl.semaphore_wait(barrier, 8)
+    pl.semaphore_wait(barrier, 13)
 
     local[0].wait()
-    start_all(down[0][1])
-    local[1].wait()
-    start_all(down[1][1])
+    for d in (4, -3, 3, -2, 2, -1, 1):
+        direct[d].start()
     local[2].wait()
     tokens_over.start()
+    local[1].wait()
+    start_all(down[1])
 
     local[3].wait()
     for h in range(4):
@@ -264,6 +271,18 @@
     start_all(up[1])
     up_hand[0].start()
 
+    def relay(step):
+        wait_all(down[step] + up[step])
+        if step < 4:
+            start_all(down[step + 1] + up[step + 1])
+        for d in (-step, step) if step < 4 else (4,):
+            start_all(sides[1][d])
+        hand(up_hand, step)
+
+    def pass_on(d):
+        direct[-d if d != 4 else 4].wait()
+        start_all(sides[0][d])
+
     for copy in local[6:11]:
         copy.wait()
     own_tab = tab[y]
@@ -274,36 +293,24 @@
     for t in range(4):
         kvb[sp, BLOCK:KV_ROWS, 128 * t : 128 * (t + 1)] = packed[32 * t : 32 * (t + 1)]
 
-    for step in range(1, 5):
-        for ch in range(2):
-            wait_all(down[ch][step])
-            if step < 4:
-                start_all(down[ch][step + 1])
-            for d in (-step, step) if step < 4 else (4,):
-                start_all(sides[ch][d])
-        if step == 1:
-            tokens_over.wait()
-            for zo in range(8):
-                columns = pl.ds(pl.multiple_of(256 * zo + 128 * c, 128), 128)
-                lhs[0:256, 128 * zo : 128 * (zo + 1)] = tk[:, columns]
-                lhs[256:512, 128 * zo : 128 * (zo + 1)] = pt[:, columns]
-        else:
-            wait_all(up[step - 1])
-            start_all(up[step])
-            hand(up_hand, step - 1)
-        if step == 2:
-            acc[...] = jnp.zeros_like(acc)
-            mbuf[...] = jnp.full_like(mbuf, -jnp.inf)
-        if step == 3:
-            for h in range(4):
-                vbuf[h, :, :, VDIM:256] = jnp.ones((16, BLOCK, 256 - VDIM), BF16)
-
-    local[5].wait()
-    for chunk in range(4):
-        start_all(out[chunk][1])
+    for d in (-1, 1, -2, 2):
+        pass_on(d)
+    tokens_over.wait()
+    for zo in range(8):
+        columns = pl.ds(pl.multiple_of(256 * zo + 128 * c, 128), 128)
+        lhs[0:256, 128 * zo : 128 * (zo + 1)] = tk[:, columns]
+        lhs[256:512, 128 * zo : 128 * (zo + 1)] = pt[:, columns]
+    for d in (-3, 3, 4):
+        pass_on(d)
+    relay(1)
+    for h in range(4):
+        vbuf[h, :, :, VDIM:256] = jnp.ones((16, BLOCK, 256 - VDIM), BF16)
+    relay(2)
+    acc[...] = jnp.zeros_like(acc)
+    mbuf[...] = jnp.full_like(mbuf, -jnp.inf)
 
     def down_project(ch):
-        for d in (-1, 1, -2, 2, -3, 3, 4):
+        for d in near:
             wait_all(sides[ch][d])
         weights = wd[:, :, RANK * ch : RANK * (ch + 1)].reshape(1024, RANK)
         part_send[ch] = dot(lhs[256:512], weights)
@@ -314,10 +321,19 @@
 
     kvb[sp, 0:BLOCK, :] = norm(down_project(0), kv_gain[...]).astype(BF16)
     start_all(ax1 + bx1[0] + by1 + ay1[0])
+    relay(3)
+    relay(4)
+    local[5].wait()
+    for chunk in range(4):
+        start_all(out[chunk][1])
+    wait_all(ax1)
+    start_all(ax2 + ay1[-1] + ay1[1])
+    wait_all(bx1[0])
+    start_all(bx2[0])
+    wait_all(by1)
+    start_all(by2 + bx1[1] + bx1[-1])
     qb[y] = norm(down_project(1), q_gain[...]).astype(BF16)
     start_all(qy1)
-    wait_all(up[4])
-    hand(up_hand, 4)
 
     def expand_queries(i):
         rows = dot(qb[i], wup[:, :, 0 : Q_WIDTH + R_WIDTH].reshape(RANK, Q_WIDTH + R_WIDTH))
@@ -335,15 +351,15 @@
             keep = low if h % 2 == 0 else jnp.logical_not(low)
             qcat[h, i, :, NOPE:256] = jnp.where(keep, pair, 0.0).astype(BF16)
 
-    def expand_keys(oy, ox):
-        o = m4(oy) * 4 + m4(ox)
-        rows = dot(kvb[o, 0:BLOCK, :], wup[:, :, Q_WIDTH + R_WIDTH :].reshape(RANK, 1024)).astype(BF16)
+    def expand_keys(oy, ox, place):
+        source, o = m4(oy) * 4 + m4(ox), m4(oy) * 4 + place
+        rows = dot(kvb[source, 0:BLOCK, :], wup[:, :, Q_WIDTH + R_WIDTH :].reshape(RANK, 1024)).astype(BF16)
         low = lax.broadcasted_iota(jnp.int32, (32, 128), 1) < 64
         for h in range(4):
             kcat[h, o, :, 0:NOPE] = rows[:, 256 * h : 256 * h + NOPE]
             vbuf[h, o, :, 0:VDIM] = rows[:, 256 * h + NOPE : 256 * (h + 1)]
         for t in range(4):
-            pair = kvb[o, BLOCK:KV_ROWS, 128 * t : 128 * (t + 1)].astype(F32)
+            pair = kvb[source, BLOCK:KV_ROWS, 128 * t : 128 * (t + 1)].astype(F32)
             turned = pltpu.roll(pair, 64, 1)
             first = jnp.where(low, pair, turned).astype(BF16)
             second = jnp.where(low, turned, pair).astype(BF16)
@@ -355,17 +371,11 @@
         dy, dxs = which
 
         def step(j, carry):
-            expand_keys(y + dy, x + dxs[0] + j * (dxs[-1] - dxs[0]))
+            expand_keys(y + dy, x + dxs[0] + j * (dxs[-1] - dxs[0]), PLACE[dxs[0]] + j)
             return carry
 
         lax.fori_loop(0, len(dxs), step, 0)
 
-    wait_all(ax1)
-    start_all(ax2 + ay1[-1] + ay1[1])
-    wait_all(bx1[0])
-    start_all(bx2[0])
-    wait_all(by1)
-    start_all(by2 + bx1[1] + bx1[-1])
     wait_all(up_hand.values())
     expand_many((0, (0,)))
     expand_queries(y)
@@ -390,22 +400,34 @@
     expand_many((0, (2,)))
     out_visit(1, 2)
 
-    def attend(i, r, masked):
+    width = BLOCK * KEY_BLOCKS
+
+    def column_of(place):
+        return m4(x + jnp.where(place == 1, 3, jnp.where(place == 2, 1, jnp.where(place == 3, 2, 0))))
+
+    def attend(i, r, sub, masked):
+        first = 4 * r + KEY_BLOCKS * sub
+
         def scores_of(h):
-            k = kcat[h, pl.ds(4 * r, 4)].reshape(1024, 256)
+            k = kcat[h, pl.ds(first, KEY_BLOCKS)].reshape(width, 256)
             return lax.dot_general(qcat[h, i], k, (((1,), (1,)), ((), ())), preferred_element_type=F32)
 
         def take(h, s):
             if masked:
-                q_pos = lax.broadcasted_iota(jnp.int32, (256, 1024), 0) + x * 256
-                k_pos = lax.broadcasted_iota(jnp.int32, (256, 1024), 1)
-                s = jnp.where(k_pos <= q_pos, s, -jnp.inf)
+                ahead = lax.broadcasted_iota(jnp.int32, (BLOCK, BLOCK), 1) - lax.broadcasted_iota(
+                    jnp.int32, (BLOCK, BLOCK), 0
+                )
+                parts = []
+                for b in range(KEY_BLOCKS):
+                    limit = BLOCK * (x - column_of(KEY_BLOCKS * sub + b))
+                    parts.append(jnp.where(ahead <= limit, s[:, BLOCK * b : BLOCK * (b + 1)], -jnp.inf))
+                s = jnp.concatenate(parts, axis=1) if KEY_BLOCKS > 1 else parts[0]
             old = mbuf[h, i]
             top = jnp.maximum(old, jnp.max(s, axis=-1, keepdims=True) * SCALE)
             p = jnp.exp2(s * SCALE - top[:, :1]).astype(BF16)
             alpha = jnp.exp2(old - top)
             mbuf[h, i] = top
-            v = vbuf[h, pl.ds(4 * r, 4)].reshape(1024, 256)
+            v = vbuf[h, pl.ds(first, KEY_BLOCKS)].reshape(width, 256)
             acc[h, i] = acc[h, i] * jnp.concatenate([alpha, alpha], axis=1) + dot(p, v)
 
         ahead = scores_of(0)
@@ -452,36 +474,64 @@
         wait_all(bx2[-1])
         expand_many((-1, (2,)))
 
-    def at_12():
-        wait_all(ay2[0])
-        expand_many((2, (0,)))
-        wait_all(ay2[-1] + ay2[1])
-        expand_many((2, (-1, 1)))
-        wait_all(ay2[2] + bx2[2])
-        expand_many((2, (2,)))
-
-    events = {1: at_1, 2: at_2, 3: at_3, 4: at_4, 6: at_6, 8: at_8, 12: at_12}
+    def send_back(d):
+        finish(m4(y + d))
+        back[d].start()
+
+    def at_last(place):
+        if place == 0:
+            for d in (1, 3):
+                pl.when(m4(y + d) < m4(y + 2))(functools.partial(send_back, d))
+            wait_all(ay2[0])
+            expand_many((2, (0,)))
+        elif place == 1:
+            wait_all(ay2[-1])
+            expand_many((2, (-1,)))
+        elif place == 2:
+            wait_all(ay2[1])
+            expand_many((2, (1,)))
+        else:
+            wait_all(ay2[2] + bx2[2])
+            expand_many((2, (2,)))
+
+    def at_sub(sub):
+        for b in range(KEY_BLOCKS):
+            at_last(KEY_BLOCKS * sub + b)
+
+    last_row = 12 * SUBS
+    events = {1: at_1, 2: at_2, 3: at_3, 4: at_4, 6: at_6, 8: at_8}
+    events = {SUBS * at: event for at, event in events.items()}
+    events.update({last_row + 4 * sub: functools.partial(at_sub, sub) for sub in range(SUBS)})
     visits = {0: (1, 3), 1: (2, 0), 2: (2, 1), 3: (2, 2), 4: (2, 3), 6: (3, 0), 7: (3, 1), 8: (3, 2), 9: (3, 3)}
 
     def slot(v, done):
-        rho, kappa = lax.div(v, 4), lax.rem(v, 4)
+        late = v >= last_row
+        rho = jnp.minimum(lax.div(v, 4 * SUBS), 3)
+        kappa = jnp.where(late, lax.rem(v, 4), lax.rem(lax.div(v, SUBS), 4))
+        sub = jnp.where(late, lax.div(v - last_row, 4), lax.rem(v, SUBS))
         swap = jnp.where(kappa == 2, 3, jnp.where(kappa == 3, 2, kappa))
         dr = jnp.where(rho == 2, 3, jnp.where(rho == 3, 2, rho))
         last = jnp.where(kappa == 0, 2, jnp.where(kappa == 2, 3, jnp.where(kappa == 3, 0, 1)))
-        r, i = m4(y + dr), m4(y + jnp.where(rho == 3, last, swap))
+        r, i = m4(y + dr), m4(y + jnp.where(late, last, swap))
         for at, event in events.items():
             pl.when(v == at)(event)
-        pl.when(i == r)(lambda: attend(i, r, True))
-        pl.when(i > r)(lambda: attend(i, r, False))
+        if KEY_BLOCKS == 1:
+            column = column_of(sub)
+            edge = jnp.logical_and(i == r, column == x)
+            whole = jnp.logical_or(i > r, jnp.logical_and(i == r, column < x))
+        else:
+            edge, whole = i == r, i > r
+        pl.when(edge)(lambda: attend(i, r, sub, True))
+        pl.when(whole)(lambda: attend(i, r, sub, False))
         active = i >= r
         for number, (step, chunk) in visits.items():
-            pl.when(jnp.logical_and(active, done == number))(functools.partial(out_visit, step, chunk))
-        pl.when(rho == 3)(lambda: finish(i))
-        for at, d in ((12, 2), (13, 1), (14, 3)):
-            pl.when(v == at)(back[d].start)
+            pl.when(jnp.logical_and(active, done == SUBS * number))(functools.partial(out_visit, step, chunk))
+        for at, d in ((0, 2), (1, 1), (2, 3)):
+            pl.when(jnp.logical_and(v == last_row + 4 * (SUBS - 1) + at, active))(functools.partial(send_back, d))
         return done + active.astype(jnp.int32)
 
-    lax.fori_loop(0, 16, slot, jnp.int32(0))
+    lax.fori_loop(0, 16 * SUBS, slot, jnp.int32(0))
+    finish(y)
 
     out_hand[0].start()
     for chunk in range(4):
@@ -509,7 +559,7 @@
     vmem_spec = pl.BlockSpec(memory_space=pltpu.VMEM)
     call = pl.pallas_call(
         kernel,
-        out_shape=jax.ShapeDtypeStruct((BLOCK, D), BF16),
+        out_shape=pltpu.VMEM((BLOCK, D), BF16),
         in_specs=[any_spec, any_spec, any_spec, any_spec, vmem_spec, vmem_spec]
         + [any_spec, any_spec, any_spec, vmem_spec, any_spec],
         out_specs=vmem_spec,
@@ -539,7 +589,7 @@
             pltpu.SemaphoreType.DMA((11,)),
         ],
         compiler_params=pltpu.CompilerParams(
-            collective_id=0, has_side_effects=True, vmem_limit_bytes=63 * 1024 * 1024
+            collective_id=0, has_side_effects=True, vmem_limit_bytes=58 * 1024 * 1024
         ),
         name="latent_attention",
     )

time: 104 us -> 101 us (0.971)
  the two profiles are of different devices: /device:TPU:1 before, /device:TPU:30 now
where the time goes in v3:
time: 101 us
  Pallas kernels  99.9 us (99%)
    pallas_call x1, Pallas kernels, body(): call(tokens[0], w_qdown, w_kvdown, w_rotary.T, q_gain[None], kv_gain[None...  99.9 us

profile of v3, /device:TPU:30, one launch (start us, length us, event | category | flops | bytes accessed | tf_op | source)
XLA Modules:
  0.0 100.8 jit_solution(1328217273853820686)
XLA Ops:
  0.0 99.9 %latent_attention.1 = bf16[256,2048]{1,0:T(8,128)(2,1)S(1)} custom-call(bf16[256,2048]{1,0:T(8,128)(2,1)} %bitcast.7, bf16[128,512]{1,0:T(8,128)(2,1)} %wq_hbm.1, bf16[128,512]{1,0:T(8,128)(2,1)} %wkv_hbm.1, bf16[64,2048]{1,0:T(8,128)(2,1)} %bitcast.8, f32[1,512]{1,0:T(1,128)} %bitcast.10, f32[1,512]{1,0:T(1,128)} %bitcast.11, bf16[32,3072]{1,0:T(8,128)(2,1)} %wqup_hbm.1, ...), custom_call_target="tpu_custom_call" | custom-call | tf_op jit(solution)/shard_map/latent_attention/pallas_call | solution.py:596
  99.9 1.0 copy.13

commit v4 on v3

--- a/solution.py
+++ b/solution.py
@@ -305,22 +305,27 @@
     relay(1)
     for h in range(4):
         vbuf[h, :, :, VDIM:256] = jnp.ones((16, BLOCK, 256 - VDIM), BF16)
+
+    def down_weights(ch):
+        return wd[:, :, RANK * ch : RANK * (ch + 1)].reshape(1024, RANK)
+
+    def down_partner(ch):
+        for d in near:
+            wait_all(sides[ch][d])
+        part_send[ch] = dot(lhs[256:512], down_weights(ch))
+        partial_over[ch].start()
+
+    def down_own(ch):
+        own = dot(lhs[0:256], down_weights(ch))
+        partial_over[ch].wait()
+        return own + part_recv[ch]
+
+    down_partner(0)
     relay(2)
+    kvb[sp, 0:BLOCK, :] = norm(down_own(0), kv_gain[...]).astype(BF16)
+    start_all(ax1 + bx1[0] + by1 + ay1[0])
     acc[...] = jnp.zeros_like(acc)
     mbuf[...] = jnp.full_like(mbuf, -jnp.inf)
-
-    def down_project(ch):
-        for d in near:
-            wait_all(sides[ch][d])
-        weights = wd[:, :, RANK * ch : RANK * (ch + 1)].reshape(1024, RANK)
-        part_send[ch] = dot(lhs[256:512], weights)
-        partial_over[ch].start()
-        own = dot(lhs[0:256], weights)
-        partial_over[ch].wait()
-        return own + part_recv[ch]
-
-    kvb[sp, 0:BLOCK, :] = norm(down_project(0), kv_gain[...]).astype(BF16)
-    start_all(ax1 + bx1[0] + by1 + ay1[0])
     relay(3)
     relay(4)
     local[5].wait()
@@ -332,7 +337,8 @@
     start_all(bx2[0])
     wait_all(by1)
     start_all(by2 + bx1[1] + bx1[-1])
-    qb[y] = norm(down_project(1), q_gain[...]).astype(BF16)
+    down_partner(1)
+    qb[y] = norm(down_own(1), q_gain[...]).astype(BF16)
     start_all(qy1)
 
     def expand_queries(i):
@@ -541,12 +547,16 @@
     def project(attended, j):
         return dot(attended, wo[pl.ds(pl.multiple_of(512 * j, 512), 512), :])
 
+    late = list(back.values()) + list(out_hand.values()) + [each for steps in out for each in steps[4]]
+    for each in moves:
+        if each not in late:
+            each.finish()
     total = project(osend[y], y)
     for d in (3, 1, 2):
         back[d].wait()
         total = total + project(orecv[m4(y - d)], m4(y - d))
     out_ref[...] = norm(total, out_gain[...]).astype(BF16)
-    for each in moves:
+    for each in late:
         each.finish()
 
 

time: 101 us -> 100 us (0.990)
  the two profiles are of different devices: /device:TPU:30 before, /device:TPU:25 now
where the time goes in v4:
time: 100 us
  Pallas kernels  99.2 us (99%)
    pallas_call x1, Pallas kernels, body(): call(tokens[0], w_qdown, w_kvdown, w_rotary.T, q_gain[None], kv_gain[None...  99.2 us

profile of v4, /device:TPU:25, one launch (start us, length us, event | category | flops | bytes accessed | tf_op | source)
XLA Modules:
  0.0 100.2 jit_solution(9854741403043039000)
XLA Ops:
  0.0 99.2 %latent_attention.1 = bf16[256,2048]{1,0:T(8,128)(2,1)S(1)} custom-call(bf16[256,2048]{1,0:T(8,128)(2,1)} %bitcast.7, bf16[128,512]{1,0:T(8,128)(2,1)} %wq_hbm.1, bf16[128,512]{1,0:T(8,128)(2,1)} %wkv_hbm.1, bf16[64,2048]{1,0:T(8,128)(2,1)} %bitcast.8, f32[1,512]{1,0:T(1,128)} %bitcast.10, f32[1,512]{1,0:T(1,128)} %bitcast.11, bf16[32,3072]{1,0:T(8,128)(2,1)} %wqup_hbm.1, ...), custom_call_target="tpu_custom_call" | custom-call | tf_op jit(solution)/shard_map/latent_attention/pallas_call | solution.py:606
  99.2 1.0 copy.13
